TPU v7x, 32 devices: a whole 2x2x4 slice. The times are simulated.
32 devices in a mesh: dp: 4 (over y, x), kv: 4 (over z), tp: 2 (over core).
Axes of the slice: x: 2, y: 2, z: 4, core: 2. Of those that a mesh axis runs over, the one named last changes fastest.
Arguments:
- tokens: bfloat16 [256, 4096], P('dp', 'kv'), may hold values from -24 to 24
- state: float32 [256, 64, 64, 64], P(('dp', 'kv'), 'tp'), may hold values from -4 to 4
- w_query: bfloat16 [4096, 4096], P('kv', 'tp'), may hold values from -0.09375 to 0.09375
- w_forget: bfloat16 [4096, 4096], P('kv', 'tp'), may hold values from -0.09375 to 0.09375
- w_input: bfloat16 [4096, 4096], P('kv', 'tp'), may hold values from -0.09375 to 0.09375
- w_gate: bfloat16 [4096, 4096], P('kv', 'tp'), may hold values from -0.09375 to 0.09375
- lower_bound: float32 [4096], P('tp'), may hold values from 0 to 0.9
- head_gain: float32 [64], replicated, may hold values from 0.1 to 1.9
- w_out: bfloat16 [4096, 4096], P('tp', 'kv'), may hold values from -0.09375 to 0.09375
- gain_one: float32 [4096], P(('kv', 'tp')), may hold values from 0.1 to 1.9
- bias_one: float32 [4096], P(('kv', 'tp')), may hold values from -2 to 2
- w_up: bfloat16 [4096, 16384], P(None, ('kv', 'tp')), may hold values from -0.09375 to 0.09375
- w_down: bfloat16 [16384, 4096], P(('kv', 'tp')), may hold values from -0.0625 to 0.0625
- gain_two: float32 [4096], P(('kv', 'tp')), may hold values from 0.1 to 1.9
- bias_two: float32 [4096], P(('kv', 'tp')), may hold values from -2 to 2
Outputs:
- result: bfloat16 [256, 4096], P('dp', ('kv', 'tp'))
- new_state: float32 [256, 64, 64, 64], P(('dp', 'kv'), 'tp')
All inputs are finite; a program needn't handle non-finite values.
Results may differ from a plain program's by a relative error of at most 0.014.
Values may be sent and summed in bfloat16 or wider, within the bound.
A program may use at most 128 MiB of HBM per device.

v0:
```python
import jax
import jax.numpy as jnp
from jax import lax
from jax.sharding import PartitionSpec as P

D = 4096


epsilon = 0.1
residual_scale = 1.68


def finish_norm(values, total, squares, width, gain, bias):
    center = total[:, None] / width
    spread = squares[:, None] / width - center * center
    return (values - center) * lax.rsqrt(spread + epsilon) * gain + bias


def per_device(
    tokens,
    state,
    w_query,
    w_forget,
    w_input,
    w_gate,
    lower_bound,
    head_gain,
    w_out,
    gain_one,
    bias_one,
    w_up,
    w_down,
    gain_two,
    bias_two,
):
    rows_own = tokens.shape[0] // lax.axis_size("kv")
    width = w_query.shape[1]
    key_size = head_gain.shape[0]
    heads_here = width // key_size
    projected = (
        lax.psum_scatter(
            jnp.concatenate(
                [
                    jnp.dot(tokens, weight, preferred_element_type=jnp.float32)
                    for weight in (w_query, w_forget, w_input, w_gate)
                ],
                axis=1,
            ),
            "kv",
            scatter_dimension=0,
            tiled=True,
        )
        .astype(jnp.bfloat16)
        .astype(jnp.float32)
    )
    shape = (rows_own, heads_here, key_size)
    query_raw = projected[:, :width].reshape(shape)
    forget_raw = projected[:, width : 2 * width].reshape(shape)
    value_raw = projected[:, 2 * width : 3 * width].reshape(shape)
    gate_raw = projected[:, 3 * width :].reshape(shape)
    bound = lower_bound.reshape(heads_here, key_size)
    forget = bound + (1.0 - bound) * jax.nn.sigmoid(forget_raw)
    keyvec = (1.0 - bound) * jax.nn.sigmoid(-forget_raw)
    query = jax.nn.silu(query_raw)
    new_state = forget[..., None] * state + keyvec[..., None] * value_raw[:, :, None, :]
    read = jnp.einsum("bhij,bhi->bhj", new_state, query, precision=lax.Precision.HIGHEST)
    read = read * lax.rsqrt(jnp.mean(jnp.square(read), axis=-1, keepdims=True) + epsilon)
    mixout = (
        (read * head_gain * jax.nn.silu(gate_raw)).reshape(rows_own, width).astype(jnp.bfloat16)
    )
    partial_value = jnp.dot(
        lax.all_gather(mixout, "kv", axis=0, tiled=True), w_out, preferred_element_type=jnp.float32
    )
    mixed = lax.psum_scatter(partial_value, "tp", scatter_dimension=1, tiled=True)
    columns = mixed.shape[1]
    own_tokens = lax.dynamic_slice_in_dim(tokens, lax.axis_index("tp") * columns, columns, 1)
    first = residual_scale * own_tokens.astype(jnp.float32) + mixed
    total, squares = lax.psum(
        (jnp.sum(first, axis=1), jnp.sum(first * first, axis=1)), ("kv", "tp")
    )
    normed_own = finish_norm(first, total, squares, D, gain_one, bias_one).astype(jnp.bfloat16)
    upper = jnp.dot(
        lax.all_gather(normed_own, ("kv", "tp"), axis=1, tiled=True),
        w_up,
        preferred_element_type=jnp.float32,
    )
    hidden = jnp.square(jax.nn.relu(upper)).astype(jnp.bfloat16)
    mlp = lax.psum_scatter(
        jnp.dot(hidden, w_down, preferred_element_type=jnp.float32).astype(jnp.bfloat16),
        ("kv", "tp"),
        scatter_dimension=1,
        tiled=True,
    ).astype(jnp.float32)
    second = residual_scale * normed_own.astype(jnp.float32) + mlp
    total_two, squares_two = lax.psum(
        (jnp.sum(second, axis=1), jnp.sum(second * second, axis=1)), ("kv", "tp")
    )
    result = finish_norm(second, total_two, squares_two, D, gain_two, bias_two).astype(jnp.bfloat16)
    return (result, new_state)


def solution(mesh):
    placed = (
        P("dp", "kv"),
        P(("dp", "kv"), "tp", None, None),
        P("kv", "tp"),
        P("kv", "tp"),
        P("kv", "tp"),
        P("kv", "tp"),
        P("tp"),
        P(),
        P("tp", "kv"),
        P(("kv", "tp")),
        P(("kv", "tp")),
        P(None, ("kv", "tp")),
        P(("kv", "tp"), None),
        P(("kv", "tp")),
        P(("kv", "tp")),
    )
    return jax.shard_map(
        per_device,
        mesh=mesh,
        in_specs=placed,
        out_specs=(P("dp", ("kv", "tp")), P(("dp", "kv"), "tp", None, None)),
        check_vma=False,
    )
```

profile of v0, /device:TPU:0, one launch (start us, length us, event | category | flops | bytes accessed | tf_op | source)
XLA Modules:
  0.0 216.7 jit_solution(5888878352963892509)
XLA Ops:
  7.2 3.2 %fusion.10 = f32[64,2048]{1,0:T(8,128)S(1)} fusion(bf16[64,1024]{1,0:T(8,128)(2,1)} %param.15, bf16[1024,2048]{1,0:T(8,128)(2,1)} %param.20), kind=kOutput, calls=%fused_computation.34 | convolution fusion | flops 268435456 | bytes 4849664 | tf_op jit(solution)/shard_map/dot_general | solution.py:44
  10.5 0.3 copy-done.1
  10.8 0.8 fusion.7
  11.6 0.4 copy-done.2
  12.0 0.8 fusion.8
  12.9 0.5 copy-done.3
  13.4 0.8 fusion.9
  14.3 1.5 pad_maximum_fusion
  15.9 46.4 %reduce-scatter.4.cloned.1.call-done = f32[16,8192]{1,0:T(8,128)} async-done(((f32[64,8192]{1,0:T(8,128)}), f32[16,8192]{1,0:T(8,128)}) %reduce-scatter.4.cloned.1.call-update) | async-done | bytes 524304 | tf_op jit(solution)/shard_map/reduce_scatter | solution.py:41
  62.3 1.1 convert_convert_fusion
  64.0 11.3 %multiply_add_fusion = f32[16,32,64,64]{3,2,1,0:T(8,128)S(1)} fusion(f32[16,32,64,64]{3,2,1,0:T(8,128)} %param.16, f32[16,32,64]{2,1,0:T(8,128)S(1)} %mul.134, f32[16,32,64]{2,1,0:T(8,128)S(1)} %get-tuple-element.16, f32[16,32,64]{2,1,0:T(8,128)S(1)} %get-tuple-element.15), kind=kLoop, calls=%fused_computation | loop fusion | flops 6291456 | bytes 17170432 | tf_op jit(solution)/shard_map/add | solution.py:65
  75.3 14.7 %fusion.11 = f32[16,32,1,64]{3,2,1,0:T(1,128)S(1)} fusion(f32[16,32,64,64]{3,2,1,0:T(8,128)S(1)} %multiply_add_fusion, f32[16,32,64,1]{2,3,1,0:T(1,128)S(1)} %bitcast.22), kind=kOutput, calls=%fused_computation.35 | convolution fusion | flops 25165824 | bytes 8650752 | tf_op jit(solution)/shard_map/bhij,bhi->bhj/dot_general | solution.py:66
  90.6 13.8 %all_gather.6 = bf16[64,2048]{1,0:T(8,128)(2,1)S(1)} all-gather(bf16[16,2048]{1,0:T(8,128)(2,1)S(1)} %convert_element_type.37), channel_id=1, replica_groups=mesh['dp'=4,'kv'=4,'tp'=2] {'kv'}, dimensions={0}, use_global_device_ids=true | all-gather | bytes 327680 | tf_op jit(solution)/shard_map/all_gather | solution.py:72
  104.4 3.7 %fusion.12 = f32[64,1024]{1,0:T(8,128)} fusion(bf16[64,2048]{1,0:T(8,128)(2,1)S(1)} %all_gather.6, bf16[2048,1024]{1,0:T(8,128)(2,1)} %param.23), kind=kOutput, calls=%fused_computation.36 | convolution fusion | flops 268435456 | bytes 4718592 | tf_op jit(solution)/shard_map/dot_general | solution.py:71
  108.2 7.2 %reduce-scatter.6.cloned.1.call-done = f32[64,512]{1,0:T(8,128)} async-done(((f32[64,1024]{1,0:T(8,128)}), f32[64,512]{1,0:T(8,128)}) %reduce-scatter.6.cloned.1.call-update) | async-done | bytes 131088 | tf_op jit(solution)/shard_map/reduce_scatter | solution.py:74
  115.4 1.0 fusion.4
  116.5 17.1 %all-reduce.1 = (f32[64]{0:T(128)S(1)}, f32[64]{0:T(128)S(1)}) all-reduce(f32[64]{0:T(128)S(1)} %get-tuple-element.3, f32[64]{0:T(128)S(1)} %get-tuple-element.2), channel_id=1, replica_groups=mesh['dp'=4,'kv'=4,'tp'=2] {'kv','tp'}, use_global_device_ids=true, to_apply=%region_6.7 | all-reduce | flops 128 | bytes 1024 | tf_op jit(solution)/shard_map/psum | solution.py:78
  133.6 1.0 add_convert_fusion.1
  134.6 15.1 %all_gather.7 = bf16[64,4096]{1,0:T(8,128)(2,1)S(1)} all-gather(bf16[64,512]{1,0:T(8,128)(2,1)S(1)} %add_convert_fusion.1), channel_id=1, replica_groups=mesh['dp'=4,'kv'=4,'tp'=2] {'kv','tp'}, dimensions={1}, use_global_device_ids=true | all-gather | bytes 589824 | tf_op jit(solution)/shard_map/all_gather | solution.py:83
  149.7 14.4 %convolution_convert_fusion = bf16[64,4096]{1,0:T(8,128)(2,1)} fusion(bf16[2048,4096]{1,0:T(8,128)(2,1)} %param.27, bf16[64,4096]{1,0:T(8,128)(2,1)S(1)} %all_gather.7, bf16[4096,2048]{1,0:T(8,128)(2,1)} %param.26), kind=kOutput, calls=%fused_computation.1 | convolution fusion | flops 2148139008 | bytes 34603008 | tf_op jit(solution)/shard_map/dot_general | solution.py:89
  164.2 29.7 %reduce-scatter.8.cloned.1.call-done = bf16[64,512]{1,0:T(8,128)(2,1)} async-done(((bf16[64,4096]{1,0:T(8,128)(2,1)}), bf16[64,512]{1,0:T(8,128)(2,1)}) %reduce-scatter.8.cloned.1.call-update) | async-done | bytes 65552 | tf_op jit(solution)/shard_map/reduce_scatter | solution.py:88
  193.8 1.0 fusion.3
  194.8 13.8 %all-reduce = (f32[64]{0:T(128)S(1)}, f32[64]{0:T(128)S(1)}) all-reduce(f32[64]{0:T(128)S(1)} %get-tuple-element.5, f32[64]{0:T(128)S(1)} %get-tuple-element.4), channel_id=1, replica_groups=mesh['dp'=4,'kv'=4,'tp'=2] {'kv','tp'}, use_global_device_ids=true, to_apply=%region_11.12 | all-reduce | flops 128 | bytes 1024 | tf_op jit(solution)/shard_map/psum | solution.py:95
  208.6 1.6 add_convert_fusion
  (41 shorter events, 1.5 us)
Async XLA Ops:
  7.2 3.3 %copy-start.4 = (bf16[64,1024]{1,0:T(8,128)(2,1)S(1)}, bf16[64,1024]{1,0:T(8,128)(2,1)}, u32[]{:S(2)}) copy-start(bf16[64,1024]{1,0:T(8,128)(2,1)} %param.15) | copy-start | bytes 393220
  7.2 55.1 %reduce-scatter.4.cloned.1.call-start = ((), (), s32[]{:S(2)}) async-start(), calls=%async_computation.3 | async-start | bytes 2621440 | tf_op jit(solution)/shard_map/reduce_scatter | solution.py:41
  7.2 3.5 %copy-start.1 = (bf16[1024,2048]{1,0:T(8,128)(2,1)S(1)}, bf16[1024,2048]{1,0:T(8,128)(2,1)}, u32[]{:S(2)}) copy-start(bf16[1024,2048]{1,0:T(8,128)(2,1)} %param.17) | copy-start | bytes 12582916
  7.2 4.8 %copy-start.2 = (bf16[1024,2048]{1,0:T(8,128)(2,1)S(1)}, bf16[1024,2048]{1,0:T(8,128)(2,1)}, u32[]{:S(2)}) copy-start(bf16[1024,2048]{1,0:T(8,128)(2,1)} %param.18) | copy-start | bytes 12582916
  10.8 2.7 %copy-start.3 = (bf16[1024,2048]{1,0:T(8,128)(2,1)S(1)}, bf16[1024,2048]{1,0:T(8,128)(2,1)}, u32[]{:S(2)}) copy-start(bf16[1024,2048]{1,0:T(8,128)(2,1)} %param.19) | copy-start | bytes 12582916
  14.3 1.6 copy-start.5
  15.8 99.7 %reduce-scatter.6.cloned.1.call-start = ((), (), s32[]{:S(2)}) async-start(), calls=%async_computation.4 | async-start | bytes 393216 | tf_op jit(solution)/shard_map/reduce_scatter | solution.py:74
  75.3 14.7 %copy-start = (f32[16,32,64,64]{3,2,1,0:T(8,128)}, f32[16,32,64,64]{3,2,1,0:T(8,128)S(1)}, u32[]{:S(2)}) copy-start(f32[16,32,64,64]{3,2,1,0:T(8,128)S(1)} %multiply_add_fusion) | copy-start | bytes 25165828
  75.3 15.0 %copy-start.10 = (f32[64]{0:T(128)S(1)}, f32[64]{0:T(128)}, u32[]{:S(2)}) copy-start(f32[64]{0:T(128)} %param.22) | copy-start | bytes 772
  90.0 43.5 %copy-start.6 = (f32[512]{0:T(512)S(1)}, f32[512]{0:T(512)}, u32[]{:S(2)}) copy-start(f32[512]{0:T(512)} %param.25) | copy-start | bytes 6148
  90.0 43.5 %copy-start.7 = (f32[512]{0:T(512)S(1)}, f32[512]{0:T(512)}, u32[]{:S(2)}) copy-start(f32[512]{0:T(512)} %param.24) | copy-start | bytes 6148
  108.2 85.7 %reduce-scatter.8.cloned.1.call-start = ((), (), s32[]{:S(2)}) async-start(), calls=%async_computation.5 | async-start | bytes 589824 | tf_op jit(solution)/shard_map/reduce_scatter | solution.py:88
  149.7 58.9 %copy-start.8 = (f32[512]{0:T(512)S(1)}, f32[512]{0:T(512)}, u32[]{:S(2)}) copy-start(f32[512]{0:T(512)} %param.29) | copy-start | bytes 6148
  149.7 58.9 %copy-start.9 = (f32[512]{0:T(512)S(1)}, f32[512]{0:T(512)}, u32[]{:S(2)}) copy-start(f32[512]{0:T(512)} %param.28) | copy-start | bytes 6148
Sparse Core Ops, SparseCore 0:
  15.9 46.3 reduce-scatter.3
  108.3 7.0 reduce-scatter.5
  164.3 29.4 reduce-scatter.7
where the time goes:
time: 217 us
  waiting for transfers between devices  83.3 us (38%)
  blocking collectives  59.8 us (28%)
  matrix products  38.6 us (18%)
  other arithmetic  18.9 us (9%)
  between operations  14 us (6%)
    reduce_scatter x1, waiting for transfers between devices, per_device(): lax.psum_scatter(jnp.concatenate([jnp.dot(tokens, weight, preferred_eleme...  46.4 us
    reduce_scatter x1, waiting for transfers between devices, per_device(): lax.psum_scatter(jnp.dot(hidden, w_down, preferred_element_type=jnp.float...  29.7 us
    psum x1, blocking collectives, per_device(): lax.psum((jnp.sum(first, axis=1), jnp.sum(first * first, axis=1)), ('kv',...  17.1 us
    all_gather x1, blocking collectives, per_device(): lax.all_gather(normed_own, ('kv', 'tp'), axis=1, tiled=True)  15.1 us
    dot_general x1, matrix products, per_device(): jnp.einsum('bhij,bhi->bhj', new_state, query, precision=lax.Precision.HIG...  14.7 us
    dot_general x1, matrix products, per_device(): jnp.dot(hidden, w_down, preferred_element_type=jnp.float32)  14.4 us
    all_gather x1, blocking collectives, per_device(): lax.all_gather(mixout, 'kv', axis=0, tiled=True)  13.8 us
    psum x1, blocking collectives, per_device(): lax.psum((jnp.sum(second, axis=1), jnp.sum(second * second, axis=1)), ('k...  13.8 us
  transfers between devices with their start and end apart: 3, of which 3 were waited for; matrix products, arithmetic and copies ran while one was open for 0% of the time, Pallas kernels for 0%

commit v1 on v0

v1 whole, which is shorter than its diff:
```python
import functools

import jax
import jax.numpy as jnp
from jax import lax
from jax.experimental import pallas as pl
from jax.experimental.pallas import tpu as pltpu
from jax.sharding import PartitionSpec as P

epsilon = 0.1
residual_scale = 1.68
MESH = pl.DeviceIdType.MESH
VMEM_BYTES = 60 * 1024 * 1024


def shifted(index, by, count):
    return lax.rem(index + by, count)


def greet(peers):
    barrier = pltpu.get_barrier_semaphore()
    for peer in peers:
        pl.semaphore_signal(barrier, inc=1, device_id=peer, device_id_type=MESH)
    return lambda: pl.semaphore_wait(barrier, len(peers))


def send(source, target, send_sem, recv_sem, peer):
    copy = pltpu.make_async_remote_copy(
        src_ref=source,
        dst_ref=target,
        send_sem=send_sem,
        recv_sem=recv_sem,
        device_id=peer,
        device_id_type=MESH,
    )
    copy.start()
    return copy


def project_kernel(
    n, chunk, tokens, wq, wf, wi, wg, out, wbuf, whole, sent, got, load_sem, send_sem, recv_sem
):
    me = lax.axis_index("kv")
    weights = (wq, wf, wi, wg)
    per = wq.shape[1] // chunk
    chunks = len(weights) * per
    rows = out.shape[0]
    peers = [{"kv": shifted(me, o, n)} for o in range(1, n)]
    wait_barrier = greet(peers)
    loads = []
    for c in range(chunks):
        load = pltpu.make_async_copy(
            weights[c // per].at[:, pl.ds((c % per) * chunk, chunk)], wbuf.at[c], load_sem.at[c]
        )
        load.start()
        loads.append(load)
    copies = {}
    for c in range(chunks):
        loads[c].wait()
        value = jnp.dot(tokens[...], wbuf[c], preferred_element_type=jnp.float32)
        value = value.reshape(n, rows, chunk)
        whole[c] = value
        sent[c] = value.astype(jnp.bfloat16)
        if c == 0:
            wait_barrier()
        for o in range(1, n):
            copies[c, o] = send(
                sent.at[c, shifted(me, o, n)],
                got.at[c, o - 1],
                send_sem.at[c, o - 1],
                recv_sem.at[c, o - 1],
                peers[o - 1],
            )
    for c in range(chunks):
        total = whole[c, me]
        for o in range(1, n):
            copies[c, o].wait_recv()
            total = total + got[c, o - 1].astype(jnp.float32)
        out[:, c * chunk : (c + 1) * chunk] = total.astype(jnp.bfloat16)
    for copy in copies.values():
        copy.wait_send()


def project(tokens, weights, n):
    count = tokens.shape[0]
    rows = count // n
    depth, width = weights[0].shape
    chunk = min(width, 1024)
    chunks = len(weights) * (width // chunk)
    return pl.pallas_call(
        functools.partial(project_kernel, n, chunk),
        out_shape=jax.ShapeDtypeStruct((rows, len(weights) * width), jnp.bfloat16),
        in_specs=[pl.BlockSpec(memory_space=pltpu.VMEM)]
        + [pl.BlockSpec(memory_space=pl.ANY)] * len(weights),
        out_specs=pl.BlockSpec(memory_space=pltpu.VMEM),
        scratch_shapes=[
            pltpu.VMEM((chunks, depth, chunk), jnp.bfloat16),
            pltpu.VMEM((chunks, n, rows, chunk), jnp.float32),
            pltpu.VMEM((chunks, n, rows, chunk), jnp.bfloat16),
            pltpu.VMEM((chunks, n - 1, rows, chunk), jnp.bfloat16),
            pltpu.SemaphoreType.DMA((chunks,)),
            pltpu.SemaphoreType.DMA((chunks, n - 1)),
            pltpu.SemaphoreType.DMA((chunks, n - 1)),
        ],
        compiler_params=pltpu.CompilerParams(
            collective_id=0, has_side_effects=True, vmem_limit_bytes=VMEM_BYTES
        ),
        name="project",
    )(tokens, *weights)


def state_kernel(state, columns, bound, rows, gain, new_state, mixout, read):
    heads = state.shape[1]
    low = bound[...]
    query_raw = columns[0, 0].astype(jnp.float32)
    forget_raw = columns[0, 1].astype(jnp.float32)
    forget = low + (1.0 - low) * jax.nn.sigmoid(forget_raw)
    keyvec = (1.0 - low) * jax.nn.sigmoid(-forget_raw)
    query = query_raw * jax.nn.sigmoid(query_raw)
    value = rows[0, 0].astype(jnp.float32)
    gate = rows[0, 1].astype(jnp.float32)
    for h in range(heads):
        here = slice(h, h + 1)
        updated = forget[:, here] * state[0, h] + keyvec[:, here] * value[here, :]
        new_state[0, h] = updated
        read[here, :] = jnp.sum(updated * query[:, here], axis=0, keepdims=True)
    whole = read[...]
    scale = lax.rsqrt(jnp.mean(whole * whole, axis=1, keepdims=True) + epsilon)
    gated = whole * scale * gain[...] * (gate * jax.nn.sigmoid(gate))
    mixout[0] = gated.astype(jnp.bfloat16)


def update_state(state, columns, bound, rows, gain):
    count, heads, size, _ = state.shape
    return pl.pallas_call(
        state_kernel,
        grid=(count,),
        out_shape=(
            jax.ShapeDtypeStruct(state.shape, jnp.float32),
            jax.ShapeDtypeStruct((count, heads, size), jnp.bfloat16),
        ),
        in_specs=[
            pl.BlockSpec((1, heads, size, size), lambda b: (b, 0, 0, 0)),
            pl.BlockSpec((1, 2, size, heads), lambda b: (b, 0, 0, 0)),
            pl.BlockSpec((size, heads), lambda b: (0, 0)),
            pl.BlockSpec((1, 2, heads, size), lambda b: (b, 0, 0, 0)),
            pl.BlockSpec((1, size), lambda b: (0, 0)),
        ],
        out_specs=(
            pl.BlockSpec((1, heads, size, size), lambda b: (b, 0, 0, 0)),
            pl.BlockSpec((1, heads, size), lambda b: (b, 0, 0)),
        ),
        scratch_shapes=[pltpu.VMEM((heads, size), jnp.float32)],
        compiler_params=pltpu.CompilerParams(vmem_limit_bytes=VMEM_BYTES),
        name="state",
    )(state, columns, bound, rows, gain)


def to_lanes(column):
    count = column.shape[0]
    diagonal = lax.broadcasted_iota(jnp.int32, (count, count), 0) == lax.broadcasted_iota(
        jnp.int32, (count, count), 1
    )
    return jnp.sum(jnp.where(diagonal, column, 0.0), axis=0, keepdims=True)


def to_sublanes(row):
    count = row.shape[1]
    diagonal = lax.broadcasted_iota(jnp.int32, (count, count), 0) == lax.broadcasted_iota(
        jnp.int32, (count, count), 1
    )
    return jnp.sum(jnp.where(diagonal, row, 0.0), axis=1, keepdims=True)


def mix_kernel(
    n,
    t,
    mixout,
    tokens,
    one,
    two,
    w_out,
    w_up,
    w_down,
    out,
    out_buf,
    up_buf,
    down_buf,
    gathered,
    part,
    part_got,
    affine,
    firsts,
    normed,
    hidden,
    near_sent,
    near_got,
    kept,
    far_sent,
    far_got,
    stats,
    load_out,
    load_up,
    load_down,
    mix_send,
    mix_recv,
    part_send,
    part_recv,
    affine_send,
    affine_recv,
    first_send,
    first_recv,
    near_send,
    near_recv,
    far_send,
    far_recv,
    stats_send,
    stats_recv,
):
    kv, tp = lax.axis_index("kv"), lax.axis_index("tp")
    count, columns = out.shape
    rows = mixout.shape[0]
    group = n * t
    me = kv * t + tp
    width = group * columns
    offsets = [(o, u) for o in range(n) for u in range(t) if (o, u) != (0, 0)]

    def at(o, u):
        return {"kv": shifted(kv, o, n), "tp": shifted(tp, u, t)}

    def block(o, u):
        return shifted(kv, o, n) * t + shifted(tp, u, t)

    def columns_of(index):
        return pl.ds(pl.multiple_of(index * columns, columns), columns)

    wait_barrier = greet([at(o, u) for o, u in offsets])

    def load(source, target, sem):
        copy = pltpu.make_async_copy(source, target, sem)
        copy.start()
        return copy

    loads_out = [
        load(w_out.at[:, columns_of(shifted(tp, u, t))], out_buf.at[u], load_out.at[u])
        for u in range(t)
    ]
    up_chunks, _, up_width = up_buf.shape
    loads_up = [
        load(w_up.at[:, pl.ds(c * up_width, up_width)], up_buf.at[c], load_up.at[c])
        for c in range(up_chunks)
    ]
    steps = [*range(1, n), 0]
    loads_down = {
        (s, u): load(
            w_down.at[:, columns_of(block(steps[s], u))], down_buf.at[s, u], load_down.at[s, u]
        )
        for s in range(n)
        for u in range(t)
    }
    gathered[kv] = mixout[...]
    affine[me] = one[...]
    wait_barrier()
    pending = []

    mixes = [
        send(mixout, gathered.at[kv], mix_send.at[o], mix_recv.at[o], at(o, 0))
        for o in range(1, n)
    ]
    affines = [
        send(one, affine.at[me], affine_send.at[o, u], affine_recv.at[o, u], at(o, u))
        for o, u in offsets
    ]
    pending += mixes + affines
    for copy in mixes:
        copy.wait_recv()
    whole = gathered[...].reshape(count, gathered.shape[2])
    parts = []
    for u in [*range(1, t), 0]:
        loads_out[u].wait()
        product = jnp.dot(whole, out_buf[u], preferred_element_type=jnp.float32)
        if u:
            part[u - 1] = product
            parts.append(
                send(
                    part.at[u - 1],
                    part_got.at[u - 1],
                    part_send.at[u - 1],
                    part_recv.at[u - 1],
                    at(0, u),
                )
            )
    pending += parts
    own_tokens = tokens[:, columns_of(tp)].astype(jnp.float32)
    first = residual_scale * own_tokens + product
    for u in range(1, t):
        parts[u - 1].wait_recv()
        first = first + part_got[u - 1]
    firsts[me] = first.astype(jnp.bfloat16)

    def pass_on(index, o, u):
        where = at(o, u) if u == 0 else at(0, u)
        copy = send(
            firsts.at[index], firsts.at[index], first_send.at[o, u], first_recv.at[o, u], where
        )
        pending.append(copy)
        return copy

    passed = {}
    for o in range(1, n):
        passed[o, 0] = pass_on(me, o, 0)
    for u in range(1, t):
        passed[0, u] = pass_on(me, 0, u)
    for copy in affines:
        copy.wait_recv()
    for o in range(1, n):
        passed[o, 0].wait_recv()
        for u in range(1, t):
            passed[o, u] = pass_on(block(n - o, 0), o, u)
    for o in range(n):
        for u in range(1, t):
            passed[o, u].wait_recv()

    total = jnp.zeros((count, 1), jnp.float32)
    for g in range(group):
        total = total + jnp.sum(firsts[g].astype(jnp.float32), axis=1, keepdims=True)
    center = total / width
    spread = jnp.zeros((count, 1), jnp.float32)
    for g in range(group):
        away = firsts[g].astype(jnp.float32) - center
        spread = spread + jnp.sum(away * away, axis=1, keepdims=True)
    scale = lax.rsqrt(spread / width + epsilon)

    def finish(values, pair):
        return ((values.astype(jnp.float32) - center) * scale * pair[0:1] + pair[1:2]).astype(
            jnp.bfloat16
        )

    for g in range(group):
        normed[:, g * columns : (g + 1) * columns] = finish(firsts[g], affine[g])
    own_normed = finish(firsts[me], one[...])

    for c in range(up_chunks):
        loads_up[c].wait()
        upper = jnp.dot(normed[...], up_buf[c], preferred_element_type=jnp.float32)
        upper = jnp.maximum(upper, 0.0)
        hidden[:, c * up_width : (c + 1) * up_width] = (upper * upper).astype(jnp.bfloat16)

    near = {}
    far = {}

    def near_sum(s):
        value = kept[s]
        for u in range(1, t):
            near[s, u].wait_recv()
            value = value + near_got[s, u - 1].astype(jnp.float32)
        return value

    def far_out(s):
        far_sent[s] = near_sum(s).astype(jnp.bfloat16)
        far[s] = send(
            far_sent.at[s], far_got.at[s], far_send.at[s], far_recv.at[s], at(steps[s], 0)
        )

    for s in range(n):
        for u in [*range(1, t), 0]:
            loads_down[s, u].wait()
            product = jnp.dot(hidden[...], down_buf[s, u], preferred_element_type=jnp.float32)
            if u:
                near_sent[s, u - 1] = product.astype(jnp.bfloat16)
                near[s, u] = send(
                    near_sent.at[s, u - 1],
                    near_got.at[s, u - 1],
                    near_send.at[s, u - 1],
                    near_recv.at[s, u - 1],
                    at(0, u),
                )
            else:
                kept[s] = product
        if s:
            far_out(s - 1)
    second = residual_scale * own_normed.astype(jnp.float32) + near_sum(n - 1)
    for s in range(n - 1):
        far[s].wait_recv()
        second = second + far_got[s].astype(jnp.float32)
    pending += list(near.values()) + list(far.values())

    sums = jnp.concatenate(
        [
            to_lanes(jnp.sum(second, axis=1, keepdims=True)),
            to_lanes(jnp.sum(second * second, axis=1, keepdims=True)),
        ],
        axis=0,
    )
    stats[0, 0:2] = sums
    tallies = []
    for i, (o, u) in enumerate(offsets):
        tallies.append(
            send(stats.at[0], stats.at[i + 1], stats_send.at[i], stats_recv.at[i], at(o, u))
        )
    pending += tallies
    for i, copy in enumerate(tallies):
        copy.wait_recv()
        sums = sums + stats[i + 1, 0:2]
    center_two = to_sublanes(sums[0:1]) / width
    spread_two = to_sublanes(sums[1:2]) / width - center_two * center_two
    result = (second - center_two) * lax.rsqrt(spread_two + epsilon) * two[0:1] + two[1:2]
    out[...] = result.astype(jnp.bfloat16)
    for copy in pending:
        copy.wait_send()


def mix(mixout, tokens, one, two, w_out, w_up, w_down, n, t):
    count = tokens.shape[0]
    rows, heads_width = mixout.shape
    columns = one.shape[1]
    depth, units = w_up.shape
    group = n * t
    up_width = min(units, 512)
    dma = pltpu.SemaphoreType.DMA
    vmem = pltpu.VMEM
    few, many = jnp.bfloat16, jnp.float32
    return pl.pallas_call(
        functools.partial(mix_kernel, n, t),
        out_shape=jax.ShapeDtypeStruct((count, columns), few),
        in_specs=[pl.BlockSpec(memory_space=pltpu.VMEM)] * 4
        + [pl.BlockSpec(memory_space=pl.ANY)] * 3,
        out_specs=pl.BlockSpec(memory_space=pltpu.VMEM),
        scratch_shapes=[
            vmem((t, heads_width, columns), few),
            vmem((units // up_width, depth, up_width), few),
            vmem((n, t, units, columns), few),
            vmem((n, rows, heads_width), few),
            vmem((t - 1, count, columns), many),
            vmem((t - 1, count, columns), many),
            vmem((group, 2, columns), many),
            vmem((group, count, columns), few),
            vmem((count, depth), few),
            vmem((count, units), few),
            vmem((n, t - 1, count, columns), few),
            vmem((n, t - 1, count, columns), few),
            vmem((n, count, columns), many),
            vmem((n, count, columns), few),
            vmem((n, count, columns), few),
            vmem((group, 8, count), many),
            dma((t,)),
            dma((units // up_width,)),
            dma((n, t)),
            dma((n,)),
            dma((n,)),
            dma((t,)),
            dma((t,)),
            dma((n, t)),
            dma((n, t)),
            dma((n, t)),
            dma((n, t)),
            dma((n, t)),
            dma((n, t)),
            dma((n,)),
            dma((n,)),
            dma((group,)),
            dma((group,)),
        ],
        compiler_params=pltpu.CompilerParams(
            collective_id=1, has_side_effects=True, vmem_limit_bytes=VMEM_BYTES
        ),
        name="mix",
    )(mixout, tokens, one, two, w_out, w_up, w_down)


def per_device(
    tokens,
    state,
    w_query,
    w_forget,
    w_input,
    w_gate,
    lower_bound,
    head_gain,
    w_out,
    gain_one,
    bias_one,
    w_up,
    w_down,
    gain_two,
    bias_two,
):
    n, t = lax.axis_size("kv"), lax.axis_size("tp")
    rows = tokens.shape[0] // n
    size = head_gain.shape[0]
    heads = w_query.shape[1] // size
    projected = project(tokens, (w_query, w_forget, w_input, w_gate), n)
    projected = projected.reshape(rows, 4, heads, size)
    new_state, mixout = update_state(
        state,
        projected[:, :2].swapaxes(2, 3),
        lower_bound.reshape(heads, size).swapaxes(0, 1),
        projected[:, 2:],
        head_gain[None, :],
    )
    result = mix(
        mixout.reshape(rows, heads * size),
        tokens,
        jnp.stack([gain_one, bias_one]),
        jnp.stack([gain_two, bias_two]),
        w_out,
        w_up,
        w_down,
        n,
        t,
    )
    return (result, new_state)


def solution(mesh):
    placed = (
        P("dp", "kv"),
        P(("dp", "kv"), "tp", None, None),
        P("kv", "tp"),
        P("kv", "tp"),
        P("kv", "tp"),
        P("kv", "tp"),
        P("tp"),
        P(),
        P("tp", "kv"),
        P(("kv", "tp")),
        P(("kv", "tp")),
        P(None, ("kv", "tp")),
        P(("kv", "tp"), None),
        P(("kv", "tp")),
        P(("kv", "tp")),
    )
    return jax.shard_map(
        per_device,
        mesh=mesh,
        in_specs=placed,
        out_specs=(P("dp", ("kv", "tp")), P(("dp", "kv"), "tp", None, None)),
        check_vma=False,
    )
```

time: 217 us -> 103 us (0.47)
  Pallas kernels: 0 us -> 93.6 us
  waiting for transfers between devices: 83.3 us -> 0 us
  blocking collectives: 59.8 us -> 0 us
  matrix products: 38.6 us -> 0 us
  other arithmetic: 18.9 us -> 0.6 us
  between operations: 14 us -> 0.68 us
  local copies, waits for them, and re-layouts: 2.04 us -> 7.19 us
    pallas_call x0 -> x3, Pallas kernels: none -> 93.6 us  [the longest x1 39.6 us: mix(): pl.pallas_call(functools.partial(mix_kernel, n, t), out_shape=jax.ShapeDt...]
    reduce_scatter x3 -> x0, waiting for transfers between devices: 83.2 us -> none  [the longest x1 46.4 us: per_device(): lax.psum_scatter(jnp.concatenate([jnp.dot(tokens, weight, preferred_eleme...]
    dot_general x7 -> x0, matrix products: 38.6 us -> none  [the longest x1 14.7 us: per_device(): jnp.einsum('bhij,bhi->bhj', new_state, query, precision=lax.Precision.HIG...]
    psum x2 -> x0, blocking collectives: 30.9 us -> none  [the longest x1 17.1 us: per_device(): lax.psum((jnp.sum(first, axis=1), jnp.sum(first * first, axis=1)), ('kv',...]
    all_gather x2 -> x0, blocking collectives: 28.9 us -> none  [the longest x1 15.1 us: per_device(): lax.all_gather(normed_own, ('kv', 'tp'), axis=1, tiled=True)]
    add x2 -> x0, other arithmetic: 11.3 us -> none  [the longest x1 11.3 us: per_device(): forget[..., None] * state + keyvec[..., None] * value_raw[:, :, None, :]]
    convert_element_type x4 -> x0, other arithmetic: 3.79 us -> none  [the longest x1 1.57 us: per_device(): finish_norm(second, total_two, squares_two, D, gain_two, bias_two)]
    reshape x2 -> x4, local copies, waits for them, and re-layouts: 0.21 us -> 3.95 us  [the longest x1 1.71 us: per_device(): mixout.reshape(rows, heads * size)]
  transfers between devices with their start and end apart: 3 -> 0, of which waited for: 3 -> 0; matrix products, arithmetic and copies ran while one was open for 0% -> 0% of each run, Pallas kernels for 0% -> 0%
where the time goes in v1:
time: 103 us; the launch traced here: 102 us
  Pallas kernels  93.6 us (91%)
  local copies, waits for them, and re-layouts  7.19 us (7%)
    pallas_call x1, Pallas kernels, mix(): pl.pallas_call(functools.partial(mix_kernel, n, t), out_shape=jax.ShapeDt...  39.6 us
    pallas_call x1, Pallas kernels, project(): pl.pallas_call(functools.partial(project_kernel, n, chunk), out_shape=jax...  31.1 us
    pallas_call x1, Pallas kernels, update_state(): pl.pallas_call(state_kernel, grid=(count,), out_shape=(jax.ShapeDtypeStru...  22.9 us

profile of v1, /device:TPU:0, one launch (start us, length us, event | category | flops | bytes accessed | tf_op | source)
XLA Modules:
  0.0 102.1 jit_solution(10745488528815226047)
XLA Ops:
  0.6 0.0 copy-start
  0.6 31.1 %project.1 = bf16[16,8192]{1,0:T(8,128)(2,1)} custom-call(bf16[64,1024]{1,0:T(8,128)(2,1)} %tokens.3, bf16[1024,2048]{1,0:T(8,128)(2,1)} %wq.1, bf16[1024,2048]{1,0:T(8,128)(2,1)} %wf.1, bf16[1024,2048]{1,0:T(8,128)(2,1)} %wi.1, bf16[1024,2048]{1,0:T(8,128)(2,1)} %wg.1), custom_call_target="tpu_custom_call" | custom-call | tf_op jit(solution)/shard_map/project/pallas_call | solution.py:90
  31.8 1.5 %reshape.13 = bf16[16,4,32,64]{3,2,1,0:T(8,128)(2,1)S(1)} reshape(bf16[16,8192]{1,0:T(8,128)(2,1)} %project.1) | data formatting | bytes 524288 | tf_op jit(solution)/shard_map/reshape | solution.py:493
  33.2 0.7 fusion
  34.0 1.0 copy.19.columns
  35.0 0.0 copy-done
  35.0 0.1 reshape.14
  35.1 0.7 copy.18
  35.8 0.0 copy-start.1
  35.8 0.0 copy-start.2
  35.8 0.0 copy-start.3
  35.8 0.0 copy-start.4
  35.8 22.9 %state.2 = (f32[16,32,64,64]{3,2,1,0:T(8,128)}, bf16[16,32,64]{2,1,0:T(8,128)(2,1)}) custom-call(f32[16,32,64,64]{3,2,1,0:T(8,128)} %state.3, bf16[16,2,64,32]{3,2,1,0:T(8,128)(2,1)} %copy.19.columns, f32[64,32]{1,0:T(8,128)} %bitcast.8, bf16[16,2,32,64]{3,2,1,0:T(8,128)(2,1)} %get-tuple-element.6.rows, f32[1,64]{1,0:T(1,128)} %bitcast.13), custom_call_target="tpu_custom_call" | custom-call | tf_op jit(solution)/shard_map/state/pallas_call | solution.py:135
  58.7 1.7 %reshape.15.mixout = bf16[16,2048]{1,0:T(8,128)(2,1)} reshape(bf16[16,32,64]{2,1,0:T(8,128)(2,1)} %get-tuple-element.4) | data formatting | bytes 131072 | tf_op jit(solution)/shard_map/reshape | solution.py:502
  60.4 0.0 copy-done.1
  60.4 0.0 copy-done.2
  60.4 0.0 copy-done.3
  60.4 0.0 copy-done.4
  60.4 0.6 pad_maximum_fusion
  61.0 39.6 %mix.1 = bf16[64,512]{1,0:T(8,128)(2,1)} custom-call(bf16[16,2048]{1,0:T(8,128)(2,1)} %reshape.15.mixout, bf16[64,1024]{1,0:T(8,128)(2,1)} %tokens.3, f32[2,512]{1,0:T(2,128)} %get-tuple-element.8.one, f32[2,512]{1,0:T(2,128)} %get-tuple-element.9.two, bf16[2048,1024]{1,0:T(8,128)(2,1)} %w_out.1, bf16[4096,2048]{1,0:T(8,128)(2,1)} %w_up.1, ...), custom_call_target="tpu_custom_call" | custom-call | tf_op jit(solution)/shard_map/mix/pallas_call | solution.py:423
  100.6 1.5 %copy.21 = bf16[64,512]{1,0:T(8,128)(2,1)} copy(bf16[64,512]{1,0:T(8,128)(2,1)} %mix.1) | data formatting | bytes 131072
Async XLA Ops:
  0.6 34.4 %copy-start = (f32[2048]{0:T(1024)S(1)}, f32[2048]{0:T(1024)}, u32[]{:S(2)}) copy-start(f32[2048]{0:T(1024)} %param.21) | copy-start | bytes 24580
  35.8 24.6 %copy-start.1 = (f32[512]{0:T(512)S(1)}, f32[512]{0:T(512)}, u32[]{:S(2)}) copy-start(f32[512]{0:T(512)} %param.25) | copy-start | bytes 6148
  35.8 24.6 %copy-start.2 = (f32[512]{0:T(512)S(1)}, f32[512]{0:T(512)}, u32[]{:S(2)}) copy-start(f32[512]{0:T(512)} %param.24) | copy-start | bytes 6148
  35.8 24.6 %copy-start.3 = (f32[512]{0:T(512)S(1)}, f32[512]{0:T(512)}, u32[]{:S(2)}) copy-start(f32[512]{0:T(512)} %param.29) | copy-start | bytes 6148
  35.8 24.6 %copy-start.4 = (f32[512]{0:T(512)S(1)}, f32[512]{0:T(512)}, u32[]{:S(2)}) copy-start(f32[512]{0:T(512)} %param.28) | copy-start | bytes 6148

commit v2 on v1

--- a/solution.py
+++ b/solution.py
@@ -2,6 +2,7 @@
 
 import jax
 import jax.numpy as jnp
+import numpy as np
 from jax import lax
 from jax.experimental import pallas as pl
 from jax.experimental.pallas import tpu as pltpu
@@ -38,30 +39,48 @@
 
 
 def project_kernel(
-    n, chunk, tokens, wq, wf, wi, wg, out, wbuf, whole, sent, got, load_sem, send_sem, recv_sem
+    n,
+    chunk,
+    size,
+    tokens,
+    bound,
+    gain,
+    wq,
+    wf,
+    wi,
+    wg,
+    columns,
+    lines,
+    wbuf,
+    whole,
+    sent,
+    got,
+    load_sem,
+    send_sem,
+    recv_sem,
 ):
     me = lax.axis_index("kv")
     weights = (wq, wf, wi, wg)
     per = wq.shape[1] // chunk
     chunks = len(weights) * per
-    rows = out.shape[0]
+    rows = lines.shape[1]
     peers = [{"kv": shifted(me, o, n)} for o in range(1, n)]
     wait_barrier = greet(peers)
-    loads = []
-    for c in range(chunks):
-        load = pltpu.make_async_copy(
+    order = [w * per + j for j in range(per) for w in range(len(weights))]
+    loads = {}
+    for c in order:
+        loads[c] = pltpu.make_async_copy(
             weights[c // per].at[:, pl.ds((c % per) * chunk, chunk)], wbuf.at[c], load_sem.at[c]
         )
-        load.start()
-        loads.append(load)
+        loads[c].start()
     copies = {}
-    for c in range(chunks):
+    for c in order:
         loads[c].wait()
         value = jnp.dot(tokens[...], wbuf[c], preferred_element_type=jnp.float32)
         value = value.reshape(n, rows, chunk)
         whole[c] = value
         sent[c] = value.astype(jnp.bfloat16)
-        if c == 0:
+        if c == order[0]:
             wait_barrier()
         for o in range(1, n):
             copies[c, o] = send(
@@ -71,28 +90,46 @@
                 recv_sem.at[c, o - 1],
                 peers[o - 1],
             )
-    for c in range(chunks):
+
+    def summed(c):
         total = whole[c, me]
         for o in range(1, n):
             copies[c, o].wait_recv()
             total = total + got[c, o - 1].astype(jnp.float32)
-        out[:, c * chunk : (c + 1) * chunk] = total.astype(jnp.bfloat16)
+        return total.astype(jnp.bfloat16).astype(jnp.float32)
+
+    heads = chunk // size
+    for j in range(per):
+        here = slice(j * chunk, (j + 1) * chunk)
+        query_raw, forget_raw, value, gate = (summed(w * per + j) for w in range(len(weights)))
+        low = bound[:, here]
+        forget = low + (1.0 - low) * jax.nn.sigmoid(forget_raw)
+        keyvec = (1.0 - low) * jax.nn.sigmoid(-forget_raw)
+        high = keyvec.astype(jnp.bfloat16).astype(jnp.float32)
+        stacked = jnp.concatenate([forget, high, keyvec - high], axis=0)
+        columns[j * heads : (j + 1) * heads] = stacked.T.reshape(heads, size, 3 * rows)
+        lines[0, :, here] = query_raw * jax.nn.sigmoid(query_raw)
+        lines[1, :, here] = value
+        lines[2, :, here] = gain[:, here] * gate * jax.nn.sigmoid(gate)
     for copy in copies.values():
         copy.wait_send()
 
 
-def project(tokens, weights, n):
+def project(tokens, bound, gain, weights, n, size):
     count = tokens.shape[0]
     rows = count // n
     depth, width = weights[0].shape
     chunk = min(width, 1024)
     chunks = len(weights) * (width // chunk)
+    vmem = pl.BlockSpec(memory_space=pltpu.VMEM)
     return pl.pallas_call(
-        functools.partial(project_kernel, n, chunk),
-        out_shape=jax.ShapeDtypeStruct((rows, len(weights) * width), jnp.bfloat16),
-        in_specs=[pl.BlockSpec(memory_space=pltpu.VMEM)]
-        + [pl.BlockSpec(memory_space=pl.ANY)] * len(weights),
-        out_specs=pl.BlockSpec(memory_space=pltpu.VMEM),
+        functools.partial(project_kernel, n, chunk, size),
+        out_shape=(
+            jax.ShapeDtypeStruct((width // size, size, 3 * rows), jnp.float32),
+            jax.ShapeDtypeStruct((3, rows, width), jnp.float32),
+        ),
+        in_specs=[vmem] * 3 + [pl.BlockSpec(memory_space=pl.ANY)] * len(weights),
+        out_specs=(vmem, vmem),
         scratch_shapes=[
             pltpu.VMEM((chunks, depth, chunk), jnp.bfloat16),
             pltpu.VMEM((chunks, n, rows, chunk), jnp.float32),
@@ -106,54 +143,78 @@
             collective_id=0, has_side_effects=True, vmem_limit_bytes=VMEM_BYTES
         ),
         name="project",
-    )(tokens, *weights)
-
-
-def state_kernel(state, columns, bound, rows, gain, new_state, mixout, read):
-    heads = state.shape[1]
-    low = bound[...]
-    query_raw = columns[0, 0].astype(jnp.float32)
-    forget_raw = columns[0, 1].astype(jnp.float32)
-    forget = low + (1.0 - low) * jax.nn.sigmoid(forget_raw)
-    keyvec = (1.0 - low) * jax.nn.sigmoid(-forget_raw)
-    query = query_raw * jax.nn.sigmoid(query_raw)
-    value = rows[0, 0].astype(jnp.float32)
-    gate = rows[0, 1].astype(jnp.float32)
+    )(tokens, bound, gain, *weights)
+
+
+def split(values):
+    high = values.astype(jnp.bfloat16)
+    return high, (values - high.astype(jnp.float32)).astype(jnp.bfloat16)
+
+
+def state_kernel(state, columns, lines, pick, new_state, mixout):
+    count, heads, size, _ = state.shape
+    row = lax.broadcasted_iota(jnp.int32, (count, size), 0)
+    gated = []
     for h in range(heads):
-        here = slice(h, h + 1)
-        updated = forget[:, here] * state[0, h] + keyvec[:, here] * value[here, :]
-        new_state[0, h] = updated
-        read[here, :] = jnp.sum(updated * query[:, here], axis=0, keepdims=True)
-    whole = read[...]
-    scale = lax.rsqrt(jnp.mean(whole * whole, axis=1, keepdims=True) + epsilon)
-    gated = whole * scale * gain[...] * (gate * jax.nn.sigmoid(gate))
-    mixout[0] = gated.astype(jnp.bfloat16)
-
-
-def update_state(state, columns, bound, rows, gain):
+
+        def turned(values):
+            return pltpu.roll(values, (heads - h) * size, 1) if h else values
+
+        query, query_rest = split(turned(lines[0])[:, :size])
+        query = jnp.concatenate([query, query, query_rest], axis=1)
+        value = turned(lines[1]).astype(jnp.bfloat16)
+        value = jnp.concatenate([value] * 3, axis=0)
+        column = columns[h]
+        factors = column.astype(jnp.bfloat16)
+        read = jnp.zeros((count, size), jnp.float32)
+        for pair in range(0, count, 2):
+            spread = jnp.concatenate([value * pick[pair], value * pick[pair + 1]], axis=1)
+            outer = jnp.dot(factors, spread, preferred_element_type=jnp.float32)
+            lanes = outer.shape[1] // 2
+            for i in range(2):
+                b = pair + i
+                added = outer[:, i * lanes : i * lanes + size]
+                updated = column[:, b : b + 1] * state[b, h] + added
+                new_state[b, h] = updated
+                high, rest = split(updated)
+                product = jnp.dot(
+                    query,
+                    jnp.concatenate([high, rest, high], axis=0),
+                    preferred_element_type=jnp.float32,
+                )
+                read = jnp.where(row == b, product, read)
+        scale = lax.rsqrt(jnp.mean(read * read, axis=1, keepdims=True) + epsilon)
+        gated.append(read * scale * turned(lines[2])[:, :size])
+    mixout[...] = jnp.concatenate(gated, axis=1).astype(jnp.bfloat16)
+
+
+def update_state(state, columns, lines):
     count, heads, size, _ = state.shape
+    lanes = 128
+    some = lanes // size
+    index = np.arange(3 * count)
+    pick = (index % count == np.arange(count)[:, None]) & (index >= count)
+    pick = jnp.asarray(pick[:, :, None] & (np.arange(lanes) < size), jnp.bfloat16)
     return pl.pallas_call(
         state_kernel,
-        grid=(count,),
+        grid=(heads // some,),
         out_shape=(
             jax.ShapeDtypeStruct(state.shape, jnp.float32),
-            jax.ShapeDtypeStruct((count, heads, size), jnp.bfloat16),
+            jax.ShapeDtypeStruct((count, heads * size), jnp.bfloat16),
         ),
         in_specs=[
-            pl.BlockSpec((1, heads, size, size), lambda b: (b, 0, 0, 0)),
-            pl.BlockSpec((1, 2, size, heads), lambda b: (b, 0, 0, 0)),
-            pl.BlockSpec((size, heads), lambda b: (0, 0)),
-            pl.BlockSpec((1, 2, heads, size), lambda b: (b, 0, 0, 0)),
-            pl.BlockSpec((1, size), lambda b: (0, 0)),
+            pl.BlockSpec((count, some, size, size), lambda h: (0, h, 0, 0)),
+            pl.BlockSpec((some, size, 3 * count), lambda h: (h, 0, 0)),
+            pl.BlockSpec((3, count, lanes), lambda h: (0, 0, h)),
+            pl.BlockSpec((count, 3 * count, lanes), lambda h: (0, 0, 0)),
         ],
         out_specs=(
-            pl.BlockSpec((1, heads, size, size), lambda b: (b, 0, 0, 0)),
-            pl.BlockSpec((1, heads, size), lambda b: (b, 0, 0)),
+            pl.BlockSpec((count, some, size, size), lambda h: (0, h, 0, 0)),
+            pl.BlockSpec((count, lanes), lambda h: (0, h)),
         ),
-        scratch_shapes=[pltpu.VMEM((heads, size), jnp.float32)],
         compiler_params=pltpu.CompilerParams(vmem_limit_bytes=VMEM_BYTES),
         name="state",
-    )(state, columns, bound, rows, gain)
+    )(state, columns, lines, pick)
 
 
 def to_lanes(column):
@@ -177,8 +238,10 @@
     t,
     mixout,
     tokens,
-    one,
-    two,
+    gain_one,
+    bias_one,
+    gain_two,
+    bias_two,
     w_out,
     w_up,
     w_down,
@@ -259,7 +322,8 @@
         for u in range(t)
     }
     gathered[kv] = mixout[...]
-    affine[me] = one[...]
+    affine[me, 0:1] = gain_one[...]
+    affine[me, 1:2] = bias_one[...]
     wait_barrier()
     pending = []
 
@@ -268,7 +332,7 @@
         for o in range(1, n)
     ]
     affines = [
-        send(one, affine.at[me], affine_send.at[o, u], affine_recv.at[o, u], at(o, u))
+        send(affine.at[me], affine.at[me], affine_send.at[o, u], affine_recv.at[o, u], at(o, u))
         for o, u in offsets
     ]
     pending += mixes + affines
@@ -338,7 +402,7 @@
 
     for g in range(group):
         normed[:, g * columns : (g + 1) * columns] = finish(firsts[g], affine[g])
-    own_normed = finish(firsts[me], one[...])
+    own_normed = finish(firsts[me], affine[me])
 
     for c in range(up_chunks):
         loads_up[c].wait()
@@ -404,16 +468,16 @@
         sums = sums + stats[i + 1, 0:2]
     center_two = to_sublanes(sums[0:1]) / width
     spread_two = to_sublanes(sums[1:2]) / width - center_two * center_two
-    result = (second - center_two) * lax.rsqrt(spread_two + epsilon) * two[0:1] + two[1:2]
+    result = (second - center_two) * lax.rsqrt(spread_two + epsilon) * gain_two[...] + bias_two[...]
     out[...] = result.astype(jnp.bfloat16)
     for copy in pending:
         copy.wait_send()
 
 
-def mix(mixout, tokens, one, two, w_out, w_up, w_down, n, t):
+def mix(mixout, tokens, affine, w_out, w_up, w_down, n, t):
     count = tokens.shape[0]
     rows, heads_width = mixout.shape
-    columns = one.shape[1]
+    columns = affine[0].shape[1]
     depth, units = w_up.shape
     group = n * t
     up_width = min(units, 512)
@@ -423,7 +487,7 @@
     return pl.pallas_call(
         functools.partial(mix_kernel, n, t),
         out_shape=jax.ShapeDtypeStruct((count, columns), few),
-        in_specs=[pl.BlockSpec(memory_space=pltpu.VMEM)] * 4
+        in_specs=[pl.BlockSpec(memory_space=pltpu.VMEM)] * 6
         + [pl.BlockSpec(memory_space=pl.ANY)] * 3,
         out_specs=pl.BlockSpec(memory_space=pltpu.VMEM),
         scratch_shapes=[
@@ -465,7 +529,7 @@
             collective_id=1, has_side_effects=True, vmem_limit_bytes=VMEM_BYTES
         ),
         name="mix",
-    )(mixout, tokens, one, two, w_out, w_up, w_down)
+    )(mixout, tokens, *affine, w_out, w_up, w_down)
 
 
 def per_device(
@@ -486,23 +550,21 @@
     bias_two,
 ):
     n, t = lax.axis_size("kv"), lax.axis_size("tp")
-    rows = tokens.shape[0] // n
     size = head_gain.shape[0]
     heads = w_query.shape[1] // size
-    projected = project(tokens, (w_query, w_forget, w_input, w_gate), n)
-    projected = projected.reshape(rows, 4, heads, size)
-    new_state, mixout = update_state(
-        state,
-        projected[:, :2].swapaxes(2, 3),
-        lower_bound.reshape(heads, size).swapaxes(0, 1),
-        projected[:, 2:],
-        head_gain[None, :],
-    )
+    columns, lines = project(
+        tokens,
+        lower_bound[None, :],
+        jnp.tile(head_gain, heads)[None, :],
+        (w_query, w_forget, w_input, w_gate),
+        n,
+        size,
+    )
+    new_state, mixout = update_state(state, columns, lines)
     result = mix(
-        mixout.reshape(rows, heads * size),
+        mixout,
         tokens,
-        jnp.stack([gain_one, bias_one]),
-        jnp.stack([gain_two, bias_two]),
+        [vector[None, :] for vector in (gain_one, bias_one, gain_two, bias_two)],
         w_out,
         w_up,
         w_down,

time: 103 us -> 122 us (1.18)
  Pallas kernels: 93.6 us -> 118 us
  local copies, waits for them, and re-layouts: 7.19 us -> 2.81 us
    pallas_call x2, Pallas kernels: 54 us -> 78.8 us  [the longest x1 47.1 us: update_state(): pl.pallas_call(state_kernel, grid=(heads // some,), out_shape=(jax.ShapeD...]
    reshape x4 -> x0, local copies, waits for them, and re-layouts: 3.95 us -> none  [the longest x1 1.71 us: per_device(): mixout.reshape(rows, heads * size)]
    another operation x0 -> x2, local copies, waits for them, and re-layouts: none -> 1.34 us  [per_device(): jnp.tile(head_gain, heads)[None, :]]
where the time goes in v2:
time: 122 us
  Pallas kernels  118 us (97%)
  local copies, waits for them, and re-layouts  2.81 us (2%)
    pallas_call x1, Pallas kernels, update_state(): pl.pallas_call(state_kernel, grid=(heads // some,), out_shape=(jax.ShapeD...  47.1 us
    pallas_call x1, Pallas kernels, mix(): pl.pallas_call(functools.partial(mix_kernel, n, t), out_shape=jax.ShapeDt...  39.6 us
    pallas_call x1, Pallas kernels, project(): pl.pallas_call(functools.partial(project_kernel, n, chunk, size), out_sha...  31.8 us

profile of v2, /device:TPU:0, one launch (start us, length us, event | category | flops | bytes accessed | tf_op | source)
XLA Modules:
  0.0 121.9 jit_solution(44058297134027735)
XLA Ops:
  0.6 0.7 tile.2
  1.3 0.7 broadcast_in_dim_tile.3.gain
  2.0 31.8 %project.1 = (f32[32,64,48]{2,1,0:T(8,128)}, f32[3,16,2048]{2,1,0:T(8,128)}) custom-call(bf16[64,1024]{1,0:T(8,128)(2,1)} %tokens.3, f32[1,2048]{1,0:T(1,128)} %bitcast.5, f32[1,2048]{1,0:T(1,128)} %broadcast_in_dim_tile.3.gain, bf16[1024,2048]{1,0:T(8,128)(2,1)} %wq.1, bf16[1024,2048]{1,0:T(8,128)(2,1)} %wf.1, bf16[1024,2048]{1,0:T(8,128)(2,1)} %wi.1, ...), custom_call_target="tpu_custom_call" | custom-call | tf_op jit(solution)/shard_map/project/pallas_call | solution.py:125
  33.8 47.1 %state.2 = (f32[16,32,64,64]{3,2,1,0:T(8,128)}, bf16[16,2048]{1,0:T(8,128)(2,1)}) custom-call(f32[16,32,64,64]{3,2,1,0:T(8,128)} %state.3, f32[32,64,48]{2,1,0:T(8,128)} %get-tuple-element.6.columns, f32[3,16,2048]{2,1,0:T(8,128)} %get-tuple-element.7.lines, bf16[16,48,128]{2,1,0:T(8,128)(2,1)} %constant.2.clone.pick), custom_call_target="tpu_custom_call" | custom-call | tf_op jit(solution)/shard_map/state/pallas_call | solution.py:198
  80.8 39.6 %mix.1 = bf16[64,512]{1,0:T(8,128)(2,1)} custom-call(bf16[16,2048]{1,0:T(8,128)(2,1)} %get-tuple-element.8.mixout, bf16[64,1024]{1,0:T(8,128)(2,1)} %tokens.3, f32[1,512]{1,0:T(1,128)} %bitcast.6, f32[1,512]{1,0:T(1,128)} %bitcast.7, f32[1,512]{1,0:T(1,128)} %bitcast.8, f32[1,512]{1,0:T(1,128)} %bitcast.9, bf16[2048,1024]{1,0:T(8,128)(2,1)} %w_out.1, ...), custom_call_target="tpu_custom_call" | custom-call | tf_op jit(solution)/shard_map/mix/pallas_call | solution.py:487
  120.4 1.5 %copy.19 = bf16[64,512]{1,0:T(8,128)(2,1)} copy(bf16[64,512]{1,0:T(8,128)(2,1)} %mix.1) | data formatting | bytes 131072

commit v3 on v2

--- a/solution.py
+++ b/solution.py
@@ -44,7 +44,6 @@
     size,
     tokens,
     bound,
-    gain,
     wq,
     wf,
     wi,
@@ -105,17 +104,19 @@
         low = bound[:, here]
         forget = low + (1.0 - low) * jax.nn.sigmoid(forget_raw)
         keyvec = (1.0 - low) * jax.nn.sigmoid(-forget_raw)
-        high = keyvec.astype(jnp.bfloat16).astype(jnp.float32)
-        stacked = jnp.concatenate([forget, high, keyvec - high], axis=0)
-        columns[j * heads : (j + 1) * heads] = stacked.T.reshape(heads, size, 3 * rows)
-        lines[0, :, here] = query_raw * jax.nn.sigmoid(query_raw)
-        lines[1, :, here] = value
-        lines[2, :, here] = gain[:, here] * gate * jax.nn.sigmoid(gate)
+        query = query_raw * jax.nn.sigmoid(query_raw)
+        for i, factor in enumerate((forget, keyvec, query)):
+            high = factor.astype(jnp.bfloat16).astype(jnp.float32)
+            stacked = jnp.concatenate([high, factor - high], axis=0)
+            turned = stacked.T.reshape(heads, size, 2 * rows).astype(jnp.bfloat16)
+            columns[i, j * heads : (j + 1) * heads] = turned
+        lines[0, :, here] = value
+        lines[1, :, here] = gate * jax.nn.sigmoid(gate)
     for copy in copies.values():
         copy.wait_send()
 
 
-def project(tokens, bound, gain, weights, n, size):
+def project(tokens, bound, weights, n, size):
     count = tokens.shape[0]
     rows = count // n
     depth, width = weights[0].shape
@@ -125,10 +126,10 @@
     return pl.pallas_call(
         functools.partial(project_kernel, n, chunk, size),
         out_shape=(
-            jax.ShapeDtypeStruct((width // size, size, 3 * rows), jnp.float32),
-            jax.ShapeDtypeStruct((3, rows, width), jnp.float32),
+            jax.ShapeDtypeStruct((3, width // size, size, 2 * rows), jnp.bfloat16),
+            jax.ShapeDtypeStruct((2, rows, width), jnp.float32),
         ),
-        in_specs=[vmem] * 3 + [pl.BlockSpec(memory_space=pl.ANY)] * len(weights),
+        in_specs=[vmem] * 2 + [pl.BlockSpec(memory_space=pl.ANY)] * len(weights),
         out_specs=(vmem, vmem),
         scratch_shapes=[
             pltpu.VMEM((chunks, depth, chunk), jnp.bfloat16),
@@ -143,58 +144,46 @@
             collective_id=0, has_side_effects=True, vmem_limit_bytes=VMEM_BYTES
         ),
         name="project",
-    )(tokens, bound, gain, *weights)
-
-
-def split(values):
-    high = values.astype(jnp.bfloat16)
-    return high, (values - high.astype(jnp.float32)).astype(jnp.bfloat16)
-
-
-def state_kernel(state, columns, lines, pick, new_state, mixout):
+    )(tokens, bound, *weights)
+
+
+def state_kernel(state, columns, lines, gain, pick, new_state, mixout, spread, value, read):
     count, heads, size, _ = state.shape
-    row = lax.broadcasted_iota(jnp.int32, (count, size), 0)
+    lanes = pick.shape[1] // count
+    factors = columns[...].reshape(3 * heads * size, 2 * count)
+    spread[...] = jnp.dot(factors, pick[...], preferred_element_type=jnp.float32)
+
+    def turned(values, h):
+        return pltpu.roll(values, (heads - h) * size, 1) if h else values
+
+    for h in range(heads):
+        value[h] = turned(lines[0], h)
     gated = []
     for h in range(heads):
-
-        def turned(values):
-            return pltpu.roll(values, (heads - h) * size, 1) if h else values
-
-        query, query_rest = split(turned(lines[0])[:, :size])
-        query = jnp.concatenate([query, query, query_rest], axis=1)
-        value = turned(lines[1]).astype(jnp.bfloat16)
-        value = jnp.concatenate([value] * 3, axis=0)
-        column = columns[h]
-        factors = column.astype(jnp.bfloat16)
-        read = jnp.zeros((count, size), jnp.float32)
-        for pair in range(0, count, 2):
-            spread = jnp.concatenate([value * pick[pair], value * pick[pair + 1]], axis=1)
-            outer = jnp.dot(factors, spread, preferred_element_type=jnp.float32)
-            lanes = outer.shape[1] // 2
-            for i in range(2):
-                b = pair + i
-                added = outer[:, i * lanes : i * lanes + size]
-                updated = column[:, b : b + 1] * state[b, h] + added
-                new_state[b, h] = updated
-                high, rest = split(updated)
-                product = jnp.dot(
-                    query,
-                    jnp.concatenate([high, rest, high], axis=0),
-                    preferred_element_type=jnp.float32,
-                )
-                read = jnp.where(row == b, product, read)
-        scale = lax.rsqrt(jnp.mean(read * read, axis=1, keepdims=True) + epsilon)
-        gated.append(read * scale * turned(lines[2])[:, :size])
+        for b in range(count):
+            forget, keyvec, query = (
+                spread[
+                    (i * heads + h) * size : (i * heads + h + 1) * size,
+                    b * lanes : b * lanes + size,
+                ]
+                for i in range(3)
+            )
+            updated = forget * state[b, h] + keyvec * value[h, b : b + 1, :size]
+            new_state[b, h] = updated
+            read[h, b : b + 1] = jnp.sum(updated * query, axis=0, keepdims=True)
+    for h in range(heads):
+        whole = read[h]
+        scale = lax.rsqrt(jnp.mean(whole * whole, axis=1, keepdims=True) + epsilon)
+        gated.append(whole * scale * gain[...] * turned(lines[1], h)[:, :size])
     mixout[...] = jnp.concatenate(gated, axis=1).astype(jnp.bfloat16)
 
 
-def update_state(state, columns, lines):
+def update_state(state, columns, lines, gain):
     count, heads, size, _ = state.shape
     lanes = 128
     some = lanes // size
-    index = np.arange(3 * count)
-    pick = (index % count == np.arange(count)[:, None]) & (index >= count)
-    pick = jnp.asarray(pick[:, :, None] & (np.arange(lanes) < size), jnp.bfloat16)
+    pick = np.arange(2 * count)[:, None] % count == np.arange(count * lanes) // lanes
+    pick = jnp.asarray(pick, jnp.bfloat16)
     return pl.pallas_call(
         state_kernel,
         grid=(heads // some,),
@@ -204,17 +193,23 @@
         ),
         in_specs=[
             pl.BlockSpec((count, some, size, size), lambda h: (0, h, 0, 0)),
-            pl.BlockSpec((some, size, 3 * count), lambda h: (h, 0, 0)),
-            pl.BlockSpec((3, count, lanes), lambda h: (0, 0, h)),
-            pl.BlockSpec((count, 3 * count, lanes), lambda h: (0, 0, 0)),
+            pl.BlockSpec((3, some, size, 2 * count), lambda h: (0, h, 0, 0)),
+            pl.BlockSpec((2, count, lanes), lambda h: (0, 0, h)),
+            pl.BlockSpec((1, size), lambda h: (0, 0)),
+            pl.BlockSpec((2 * count, count * lanes), lambda h: (0, 0)),
         ],
         out_specs=(
             pl.BlockSpec((count, some, size, size), lambda h: (0, h, 0, 0)),
             pl.BlockSpec((count, lanes), lambda h: (0, h)),
         ),
+        scratch_shapes=[
+            pltpu.VMEM((3 * some * size, count * lanes), jnp.float32),
+            pltpu.VMEM((some, count, lanes), jnp.float32),
+            pltpu.VMEM((some, count, size), jnp.float32),
+        ],
         compiler_params=pltpu.CompilerParams(vmem_limit_bytes=VMEM_BYTES),
         name="state",
-    )(state, columns, lines, pick)
+    )(state, columns, lines, gain, pick)
 
 
 def to_lanes(column):
@@ -551,16 +546,14 @@
 ):
     n, t = lax.axis_size("kv"), lax.axis_size("tp")
     size = head_gain.shape[0]
-    heads = w_query.shape[1] // size
     columns, lines = project(
         tokens,
         lower_bound[None, :],
-        jnp.tile(head_gain, heads)[None, :],
         (w_query, w_forget, w_input, w_gate),
         n,
         size,
     )
-    new_state, mixout = update_state(state, columns, lines)
+    new_state, mixout = update_state(state, columns, lines, head_gain[None, :])
     result = mix(
         mixout,
         tokens,

time: 122 us -> 95 us (0.78)
  Pallas kernels: 118 us -> 92.3 us
  local copies, waits for them, and re-layouts: 2.81 us -> 1.47 us
    pallas_call x1, Pallas kernels: 47.1 us -> 20.7 us  [update_state(): pl.pallas_call(state_kernel, grid=(heads // some,), out_shape=(jax.ShapeD...]
    another operation x2 -> x0, local copies, waits for them, and re-layouts: 1.34 us -> none  [per_device(): jnp.tile(head_gain, heads)[None, :]]
where the time goes in v3:
time: 95 us; the launch traced here: 94.4 us
  Pallas kernels  92.3 us (97%)
  local copies, waits for them, and re-layouts  1.47 us (2%)
    pallas_call x1, Pallas kernels, mix(): pl.pallas_call(functools.partial(mix_kernel, n, t), out_shape=jax.ShapeDt...  39.5 us
    pallas_call x1, Pallas kernels, project(): pl.pallas_call(functools.partial(project_kernel, n, chunk, size), out_sha...  32 us
    pallas_call x1, Pallas kernels, update_state(): pl.pallas_call(state_kernel, grid=(heads // some,), out_shape=(jax.ShapeD...  20.7 us

profile of v3, /device:TPU:0, one launch (start us, length us, event | category | flops | bytes accessed | tf_op | source)
XLA Modules:
  0.0 94.4 jit_solution(3268270017217212174)
XLA Ops:
  0.6 32.0 %project.1 = (bf16[3,32,64,32]{3,2,1,0:T(8,128)(2,1)}, f32[2,16,2048]{2,1,0:T(8,128)}) custom-call(bf16[64,1024]{1,0:T(8,128)(2,1)} %tokens.3, f32[1,2048]{1,0:T(1,128)} %bitcast.6, bf16[1024,2048]{1,0:T(8,128)(2,1)} %wq.1, bf16[1024,2048]{1,0:T(8,128)(2,1)} %wf.1, bf16[1024,2048]{1,0:T(8,128)(2,1)} %wi.1, bf16[1024,2048]{1,0:T(8,128)(2,1)} %wg.1), custom_call_target="tpu_custom_call" | custom-call | tf_op jit(solution)/shard_map/project/pallas_call | solution.py:126
  32.6 20.7 %state.2 = (f32[16,32,64,64]{3,2,1,0:T(8,128)}, bf16[16,2048]{1,0:T(8,128)(2,1)}) custom-call(f32[16,32,64,64]{3,2,1,0:T(8,128)} %state.3, bf16[3,32,64,32]{3,2,1,0:T(8,128)(2,1)} %get-tuple-element.6.columns, f32[2,16,2048]{2,1,0:T(8,128)} %get-tuple-element.7.lines, f32[1,64]{1,0:T(1,128)} %bitcast.11, bf16[32,2048]{1,0:T(8,128)(2,1)} %constant.2.clone.pick), custom_call_target="tpu_custom_call" | custom-call | tf_op jit(solution)/shard_map/state/pallas_call | solution.py:187
  53.4 39.5 %mix.1 = bf16[64,512]{1,0:T(8,128)(2,1)} custom-call(bf16[16,2048]{1,0:T(8,128)(2,1)} %get-tuple-element.8.mixout, bf16[64,1024]{1,0:T(8,128)(2,1)} %tokens.3, f32[1,512]{1,0:T(1,128)} %bitcast.7, f32[1,512]{1,0:T(1,128)} %bitcast.8, f32[1,512]{1,0:T(1,128)} %bitcast.9, f32[1,512]{1,0:T(1,128)} %bitcast.10, bf16[2048,1024]{1,0:T(8,128)(2,1)} %w_out.1, ...), custom_call_target="tpu_custom_call" | custom-call | tf_op jit(solution)/shard_map/mix/pallas_call | solution.py:482
  92.9 1.5 %copy.19 = bf16[64,512]{1,0:T(8,128)(2,1)} copy(bf16[64,512]{1,0:T(8,128)(2,1)} %mix.1) | data formatting | bytes 131072
